TPU v7x, 32 devices: a whole 2x2x4 slice. The times are simulated.
32 devices in a mesh: sp: 8 (over z, x), dp: 4 (over y, core).
Axes of the slice: x: 2, y: 2, z: 4, core: 2. Of those that a mesh axis runs over, the one named last changes fastest.
Arguments:
- hidden_in: bfloat16 [4, 1024, 2048], P('dp', 'sp'), may hold values from -6 to 6
- mix_cotangent: bfloat16 [4, 1024, 4096], P('dp', 'sp'), may hold values from -0.119628906 to 0.119628906
- query_weight: bfloat16 [2048, 4096], P('dp', 'sp'), may hold values from -0.125 to 0.125
- key_weight: bfloat16 [2048, 4096], P('dp', 'sp'), may hold values from -0.125 to 0.125
- value_weight: bfloat16 [2048, 4096], P('dp', 'sp'), may hold values from -0.125 to 0.125
- decay_log: float32 [16], P('sp'), may hold values from -0.034 to -0.00029296875, as said below
Outputs:
- grad_hidden: bfloat16 [4, 1024, 2048], P('dp', 'sp')
- grad_query: float32 [2048, 4096], P('dp', 'sp')
- grad_key: float32 [2048, 4096], P('dp', 'sp')
- grad_value: float32 [2048, 4096], P('dp', 'sp')
Inputs may be any that keep to these rules, and one draw needn't show every extreme that they name: Each head's decay_log is negative.
All inputs are finite; a program needn't handle non-finite values.
Results may differ from a plain program's by a relative error of at most 0.015.
Values may be sent and summed in bfloat16 or wider, within the bound.
A program may use at most 64 MiB of HBM per device.

v0:
```python
import jax
import jax.numpy as jnp
from jax import lax
from jax.sharding import PartitionSpec as P

BLOCK = 128


def head_grads(queries, key_rows, values, cotangent, log_rate):
    length = queries.shape[0]
    head_dim = queries.shape[1]
    blocks = length // BLOCK
    scale = head_dim ** (-0.5)
    keys_scaled = (key_rows.astype(jnp.float32) * scale).astype(jnp.bfloat16)
    offsets = jnp.arange(BLOCK, dtype=jnp.float32)
    spread = offsets[:, None] - offsets[None, :]
    inner_decay = jnp.where(spread >= 0, jnp.exp(log_rate * jnp.maximum(spread, 0.0)), 0.0)
    query_decay = jnp.exp(log_rate * (offsets + 1.0))
    key_decay = jnp.exp(log_rate * (BLOCK - 1.0 - offsets))
    block_decay = jnp.exp(log_rate * BLOCK)

    def split_blocks(series):
        return series.reshape(blocks, BLOCK, series.shape[-1])

    def forward(carried, inputs):
        query_block, key_block, value_block, grad_block = inputs
        mixed = (
            jnp.dot(grad_block, value_block.T, preferred_element_type=jnp.float32) * inner_decay
        ).astype(jnp.bfloat16)
        within = jnp.dot(mixed, key_block, preferred_element_type=jnp.float32)
        across = (
            jnp.dot(grad_block, carried.astype(jnp.bfloat16).T, preferred_element_type=jnp.float32)
            * query_decay[:, None]
        )
        weighted = (key_block.astype(jnp.float32) * key_decay[:, None]).astype(jnp.bfloat16)
        updated = carried * block_decay + jnp.dot(
            weighted.T, value_block, preferred_element_type=jnp.float32
        )
        return (updated, (within + across, mixed))

    def backward(carried, inputs):
        query_block, key_block, value_block, grad_block, mixed = inputs
        scores = (
            jnp.dot(query_block, key_block.T, preferred_element_type=jnp.float32) * inner_decay
        ).astype(jnp.bfloat16)
        state_bf = carried.astype(jnp.bfloat16)
        grad_v = (
            jnp.dot(scores.T, grad_block, preferred_element_type=jnp.float32)
            + jnp.dot(key_block, state_bf, preferred_element_type=jnp.float32) * key_decay[:, None]
        )
        grad_k = (
            jnp.dot(mixed.T, query_block, preferred_element_type=jnp.float32)
            + jnp.dot(value_block, state_bf.T, preferred_element_type=jnp.float32)
            * key_decay[:, None]
        ) * scale
        weighted = (query_block.astype(jnp.float32) * query_decay[:, None]).astype(jnp.bfloat16)
        updated = carried * block_decay + jnp.dot(
            weighted.T, grad_block, preferred_element_type=jnp.float32
        )
        return (updated, (grad_k, grad_v))

    inputs = (
        split_blocks(queries),
        split_blocks(keys_scaled),
        split_blocks(values),
        split_blocks(cotangent),
    )
    initial = jnp.zeros((head_dim, values.shape[-1]), jnp.float32)
    final_state, (grad_q, mixed_all) = lax.scan(forward, initial, inputs)
    final_back, (grad_k, grad_v) = lax.scan(backward, initial, inputs + (mixed_all,), reverse=True)
    return (grad_q.reshape(length, -1), grad_k.reshape(length, -1), grad_v.reshape(length, -1))


def group_grads(log_rates, queries, key_rows, values, cotangent):
    length = queries.shape[0]
    head_count = log_rates.shape[0]

    def by_head(series):
        return series.reshape(length, head_count, -1).transpose(1, 0, 2)

    def to_rows(series):
        return series.transpose(1, 0, 2).reshape(length, -1)

    grad_q, grad_k, grad_v = jax.vmap(head_grads)(
        by_head(queries), by_head(key_rows), by_head(values), by_head(cotangent), log_rates
    )
    return jnp.concatenate((to_rows(grad_q), to_rows(grad_k), to_rows(grad_v)), axis=1).astype(
        jnp.bfloat16
    )


def body(hidden_in, mix_cotangent, query_weight, key_weight, value_weight, decay_log):
    own_rows = hidden_in[0]
    columns = query_weight.shape[1]
    stacked = jnp.stack((query_weight, key_weight, value_weight), axis=1)
    gathered = lax.all_gather(stacked, "dp", axis=0, tiled=True)
    weights = gathered.reshape(gathered.shape[0], 3 * columns)
    cotangent = lax.all_to_all(mix_cotangent[0], "sp", split_axis=1, concat_axis=0, tiled=True)
    all_rows = lax.all_gather(own_rows, "sp", axis=0, tiled=True)
    projected = jnp.dot(all_rows, weights, preferred_element_type=jnp.float32).astype(jnp.bfloat16)
    gradients = group_grads(
        decay_log,
        projected[:, :columns],
        projected[:, columns : 2 * columns],
        projected[:, 2 * columns :],
        cotangent,
    )
    input_sum = lax.psum_scatter(
        lax.dot_general(
            gradients, weights, (((1,), (1,)), ((), ())), preferred_element_type=jnp.float32
        ).astype(jnp.bfloat16),
        "sp",
        scatter_dimension=0,
        tiled=True,
    )
    grad_hidden = input_sum[None]
    summed = lax.psum_scatter(
        lax.dot_general(
            all_rows, gradients, (((0,), (0,)), ((), ())), preferred_element_type=jnp.float32
        ).astype(jnp.bfloat16),
        "dp",
        scatter_dimension=0,
        tiled=True,
    ).astype(jnp.float32) / lax.axis_size("dp")
    return (
        grad_hidden,
        summed[:, :columns],
        summed[:, columns : 2 * columns],
        summed[:, 2 * columns :],
    )


def solution(mesh):
    placed = (
        P("dp", "sp", None),
        P("dp", "sp", None),
        P("dp", "sp"),
        P("dp", "sp"),
        P("dp", "sp"),
        P("sp"),
    )
    return jax.shard_map(
        body,
        mesh=mesh,
        in_specs=placed,
        out_specs=(P("dp", "sp", None), P("dp", "sp"), P("dp", "sp"), P("dp", "sp")),
        check_vma=False,
    )
```

profile of v0, /device:TPU:0, one launch (start us, length us, event | category | flops | bytes accessed | tf_op | source)
XLA Modules:
  0.0 433.3 jit_solution(4035622993823633458)
XLA Ops:
  14.4 7.3 %all-to-all-start = ((bf16[128,8,512]{0,2,1:T(8,128)(2,1)}), bf16[128,8,512]{0,2,1:T(8,128)(2,1)S(1)}, u32[]{:S(2)}, u32[]{:S(2)}) async-start(bf16[128,8,512]{0,2,1:T(8,128)(2,1)} %bitcast.14), calls=%async_computation | async-start | bytes 2097152 | tf_op jit(solution)/shard_map/all_to_all | solution.py:98
  21.9 42.4 %all-to-all-done = bf16[128,8,512]{0,2,1:T(8,128)(2,1)S(1)} async-done(((bf16[128,8,512]{0,2,1:T(8,128)(2,1)}), bf16[128,8,512]{0,2,1:T(8,128)(2,1)S(1)}, u32[]{:S(2)}, u32[]{:S(2)}) %all-to-all-start) | async-done | bytes 1048608 | tf_op jit(solution)/shard_map/all_to_all | solution.py:98
  66.1 39.1 %all-gather.6.cloned.1.call-done = bf16[1,1024,2048]{2,1,0:T(8,128)(2,1)} async-done(((bf16[1,128,2048]{2,1,0:T(8,128)(2,1)}), bf16[1,1024,2048]{2,1,0:T(8,128)(2,1)}) %all-gather.6.cloned.1.call-update) | async-done | bytes 4194320 | tf_op jit(solution)/shard_map/all_gather | solution.py:99
  105.1 46.5 %all-gather.4.cloned.1.call-done = bf16[2048,3,512]{0,2,1:T(8,128)(2,1)} async-done(((bf16[512,3,512]{0,2,1:T(8,128)(2,1)}), bf16[2048,3,512]{0,2,1:T(8,128)(2,1)}) %all-gather.4.cloned.1.call-update) | async-done | bytes 6291472 | tf_op jit(solution)/shard_map/all_gather | solution.py:96
  151.6 10.1 %fusion.93 = bf16[1024,1536]{0,1:T(8,128)(2,1)S(1)} fusion(bf16[2048,1536]{0,1:T(8,128)(2,1)} %bitcast.197, bf16[1,1024,2048]{2,1,0:T(8,128)(2,1)} %all-gather.6.cloned.1.call-done), kind=kOutput, calls=%fused_computation.98 | convolution fusion | flops 6444023808 | bytes 13631488 | tf_op jit(solution)/shard_map/dot_general | solution.py:100
  163.4 2.3 copy.54
  165.6 2.3 copy.59
  171.6 33.4 %while.38 = (s32[]{:T(128)}, f32[2,256,256]{2,1,0:T(8,128)S(1)}, bf16[8,2,128,256]{3,2,0,1:T(8,128)(2,1)}, bf16[8,2,128,128]{3,2,1,0:T(8,128)(2,1)}, f32[2]{0:T(...) while((s32[]{:T(128)}, f32[2,256,256]{2,1,0:T(8,128)S(1)}, ...), condition=%wide.region_1.2_spmd.clone.clone.clone, body=%wide.region_0.1_spmd.clone.clone.clone.sunk | while | flops 101646848 | bytes 3434148 | solution.py:69
  175.8 1.7 bitcast_dynamic-update-slice_fusion.2
  205.0 2.3 copy.63
  209.4 52.0 %while.39 = (s32[]{:T(128)}, f32[2,256,256]{2,1,0:T(8,128)S(1)}, bf16[8,2,128,256]{3,2,0,1:T(8,128)(2,1)}, bf16[8,2,128,256]{3,2,0,1:T(8,128)(2,1)}, f32[2]{0:T(...) while((s32[]{:T(128)}, f32[2,256,256]{2,1,0:T(8,128)S(1)}, ...), condition=%wide.region_3.4_spmd.clone.clone.clone, body=%wide.region_2.3_spmd.clone.clone.clone.sunk | while | flops 152306176 | bytes 4880578 | solution.py:70
  212.8 1.8 fusion.138
  219.3 1.8 fusion.138
  225.8 1.8 fusion.138
  232.3 1.8 fusion.138
  238.8 1.8 fusion.138
  245.4 1.8 fusion.138
  251.9 1.8 fusion.138
  258.4 1.8 fusion.138
  265.9 10.4 %fusion.86 = bf16[2048,1536]{0,1:T(8,128)(2,1)} fusion(bf16[1,1024,2048]{2,1,0:T(8,128)(2,1)} %all-gather.6.cloned.1.call-done, bf16[1024,512]{0,1:T(8,128)(2,1)S(1)} %bitcast.193, bf16[1024,512]{0,1:T(8,128)(2,1)S(1)} %bitcast.191, bf16[1024,512]{0,1:T(8,128)(2,1)} %bitcast.195), kind=kOutput, calls=%fused_computation.92 | convolution fusion | flops 6455033856 | bytes 13631488 | tf_op jit(solution)/shard_map/dot_general | solution.py:118
  277.5 11.1 %convolution_convert_fusion.1 = bf16[1024,2048]{1,0:T(8,128)(2,1)} fusion(bf16[2048,1536]{0,1:T(8,128)(2,1)} %bitcast.198, bf16[1024,512]{0,1:T(8,128)(2,1)S(1)} %bitcast.194, bf16[1024,512]{0,1:T(8,128)(2,1)S(1)} %bitcast.192, bf16[1024,512]{0,1:T(8,128)(2,1)S(1)} %bitcast.196), kind=kOutput, calls=%fused_computation.96 | convolution fusion | flops 6453985280 | bytes 13631488 | tf_op jit(solution)/shard_map/dot_general | solution.py:109
  288.7 45.7 %reduce-scatter.5.cloned.1.call-done = bf16[512,1536]{0,1:T(8,128)(2,1)} async-done(((bf16[2048,1536]{0,1:T(8,128)(2,1)}), bf16[512,1536]{0,1:T(8,128)(2,1)}) %reduce-scatter.5.cloned.1.call-update) | async-done | bytes 1572880 | tf_op jit(solution)/shard_map/reduce_scatter | solution.py:117
  334.3 1.8 convert_multiply_fusion
  340.4 86.3 %reduce-scatter.3.cloned.1.call-done = bf16[128,2048]{1,0:T(8,128)(2,1)} async-done(((bf16[1024,2048]{1,0:T(8,128)(2,1)}), bf16[128,2048]{1,0:T(8,128)(2,1)}) %reduce-scatter.3.cloned.1.call-update) | async-done | bytes 524304 | tf_op jit(solution)/shard_map/reduce_scatter | solution.py:108
  (125 shorter events, 95.1 us)
Async XLA Ops:
  7.2 5.9 %copy-start.1 = (bf16[1,128,4096]{2,1,0:T(8,128)(2,1)S(1)}, bf16[1,128,4096]{2,1,0:T(8,128)(2,1)}, u32[]{:S(2)}) copy-start(bf16[1,128,4096]{2,1,0:T(8,128)(2,1)} %param.11) | copy-start | bytes 3145732
  7.2 98.0 %all-gather.6.cloned.1.call-start = ((), (), s32[]{:S(2)}) async-start(), calls=%async_computation.6 | async-start | bytes 4718592 | tf_op jit(solution)/shard_map/all_gather | solution.py:99
  7.9 143.7 %all-gather.4.cloned.1.call-start = ((), (), s32[]{:S(2)}) async-start(), calls=%async_computation.3 | async-start | bytes 7864320 | tf_op jit(solution)/shard_map/all_gather | solution.py:96
  11.7 10.1 %copy-start.3 = (f32[2]{0:T(128)S(1)}, f32[2]{0:T(128)}, u32[]{:S(2)}) copy-start(f32[2]{0:T(128)} %param.15) | copy-start | bytes 28
  14.4 49.9 %all-to-all-start = ((bf16[128,8,512]{0,2,1:T(8,128)(2,1)}), bf16[128,8,512]{0,2,1:T(8,128)(2,1)S(1)}, u32[]{:S(2)}, u32[]{:S(2)}) async-start(bf16[128,8,512]{0,2,1:T(8,128)(2,1)} %bitcast.14), calls=%async_computation | async-start | bytes 2097152 | tf_op jit(solution)/shard_map/all_to_all | solution.py:98
  21.7 312.7 %reduce-scatter.5.cloned.1.call-start = ((), (), s32[]{:S(2)}) async-start(), calls=%async_computation.5 | async-start | bytes 7864320 | tf_op jit(solution)/shard_map/reduce_scatter | solution.py:117
  261.4 3.1 copy-start
  276.3 1.2 copy-start.2
  276.3 150.4 %reduce-scatter.3.cloned.1.call-start = ((), (), s32[]{:S(2)}) async-start(), calls=%async_computation.4 | async-start | bytes 4718592 | tf_op jit(solution)/shard_map/reduce_scatter | solution.py:108
Sparse Core Ops, SparseCore 0:
  10.1 94.9 all-gather.5
  106.7 44.8 all-gather.3
  276.4 57.8 reduce-scatter.4
  338.4 88.2 reduce-scatter.2
where the time goes:
time: 435 us; the launch traced here: 433 us
  waiting for transfers between devices  261 us (60%)
  matrix products  115 us (26%)
  local copies, waits for them, and re-layouts  30.6 us (7%)
  between operations  14 us (3%)
  starting transfers between devices  7.62 us (2%)
  other arithmetic  4.64 us (1%)
    reduce_scatter x1, waiting for transfers between devices, body(): lax.psum_scatter(lax.dot_general(gradients, weights, (((1,), (1,)), ((),...  86.3 us
    all_gather x1, waiting for transfers between devices, body(): gathered = lax.all_gather(stacked, 'dp', axis=0, tiled=True)  46.5 us
    reduce_scatter x1, waiting for transfers between devices, body(): lax.psum_scatter(lax.dot_general(all_rows, gradients, (((0,), (0,)), ((),...  45.7 us
    all_to_all x1, waiting for transfers between devices, body(): lax.all_to_all(mix_cotangent[0], 'sp', split_axis=1, concat_axis=0, tiled...  42.4 us
    all_gather x1, waiting for transfers between devices, body(): all_rows = lax.all_gather(own_rows, 'sp', axis=0, tiled=True)  39.1 us
    dot_general x8, matrix products, backward(): jnp.dot(value_block, state_bf.T, preferred_element_type=jnp.float32)  14.4 us
    dot_general x8, matrix products, forward(): jnp.dot(grad_block, value_block.T, preferred_element_type=jnp.float32)  13.9 us
    unnamed x18, local copies, waits for them, and re-layouts  13.7 us
  transfers between devices with their start and end apart: 5, of which 5 were waited for; matrix products, arithmetic and copies ran while one was open for 6% of the time, Pallas kernels for 0%

commit v1 on v0

--- a/solution.py
+++ b/solution.py
@@ -4,6 +4,19 @@
 from jax.sharding import PartitionSpec as P
 
 BLOCK = 128
+
+
+def edit_units(inp):
+    ndev = lax.axis_size("dp")
+    local_next = sorted(((at, (at + 1) % ndev) for at in range(ndev)))
+    val = inp
+    vals = [val]
+    i = 1
+    while i < ndev:
+        val = lax.ppermute(val, "dp", local_next)
+        vals.insert(0, val)
+        i = i + 1
+    return jnp.roll(jnp.concatenate(vals, 0), (lax.axis_index("dp") + 1) * inp.shape[0], axis=0)
 
 
 def head_grads(queries, key_rows, values, cotangent, log_rate):
@@ -93,7 +106,7 @@
     own_rows = hidden_in[0]
     columns = query_weight.shape[1]
     stacked = jnp.stack((query_weight, key_weight, value_weight), axis=1)
-    gathered = lax.all_gather(stacked, "dp", axis=0, tiled=True)
+    gathered = edit_units(stacked)
     weights = gathered.reshape(gathered.shape[0], 3 * columns)
     cotangent = lax.all_to_all(mix_cotangent[0], "sp", split_axis=1, concat_axis=0, tiled=True)
     all_rows = lax.all_gather(own_rows, "sp", axis=0, tiled=True)

time: 435 us -> 396 us (0.910)
  waiting for transfers between devices: 261 us -> 205 us
  local copies, waits for them, and re-layouts: 30.6 us -> 48.5 us
    all_gather x1 -> x0, waiting for transfers between devices: 46.5 us -> none  [body(): gathered = lax.all_gather(stacked, 'dp', axis=0, tiled=True)]
    all_gather x1, waiting for transfers between devices: 39.1 us -> 0.01 us  [body(): all_rows = lax.all_gather(own_rows, 'sp', axis=0, tiled=True)]
    ppermute x0 -> x3, waiting for transfers between devices: none -> 32.4 us  [edit_units(): val = lax.ppermute(val, 'dp', local_next)]
    unnamed x18 -> x28, local copies, waits for them, and re-layouts: 13.7 us -> 25 us
    all_to_all x1, waiting for transfers between devices: 42.4 us -> 34.9 us  [body(): lax.all_to_all(mix_cotangent[0], 'sp', split_axis=1, concat_axis=0, tiled...]
    reduce_scatter x1, waiting for transfers between devices: 45.7 us -> 50.2 us  [body(): lax.psum_scatter(lax.dot_general(all_rows, gradients, (((0,), (0,)), ((),...]
  transfers between devices with their start and end apart: 5 -> 7, of which waited for: 5 -> 5; matrix products, arithmetic and copies ran while one was open for 6% -> 11% of each run, Pallas kernels for 0% -> 0%
where the time goes in v1:
time: 396 us; the launch traced here: 394 us
  waiting for transfers between devices  205 us (52%)
  matrix products  115 us (29%)
  local copies, waits for them, and re-layouts  48.5 us (12%)
  between operations  14 us (4%)
  starting transfers between devices  7.25 us (2%)
  other arithmetic  3.96 us (1%)
    reduce_scatter x1, waiting for transfers between devices, body(): lax.psum_scatter(lax.dot_general(gradients, weights, (((1,), (1,)), ((),...  86.4 us
    reduce_scatter x1, waiting for transfers between devices, body(): lax.psum_scatter(lax.dot_general(all_rows, gradients, (((0,), (0,)), ((),...  50.2 us
    all_to_all x1, waiting for transfers between devices, body(): lax.all_to_all(mix_cotangent[0], 'sp', split_axis=1, concat_axis=0, tiled...  34.9 us
    ppermute x3, waiting for transfers between devices, edit_units(): val = lax.ppermute(val, 'dp', local_next)  32.4 us
    unnamed x28, local copies, waits for them, and re-layouts  25 us
    dot_general x8, matrix products, backward(): jnp.dot(value_block, state_bf.T, preferred_element_type=jnp.float32)  14.4 us
    dot_general x8, matrix products, forward(): jnp.dot(grad_block, value_block.T, preferred_element_type=jnp.float32)  13.9 us
    dot_general x1, matrix products, body(): lax.dot_general(gradients, weights, (((1,), (1,)), ((), ())), preferred_e...  11.1 us
  transfers between devices with their start and end apart: 7, of which 5 were waited for; matrix products, arithmetic and copies ran while one was open for 11% of the time, Pallas kernels for 0%

profile of v1, /device:TPU:0, one launch (start us, length us, event | category | flops | bytes accessed | tf_op | source)
XLA Modules:
  0.0 394.3 jit_solution(9738966738681231560)
XLA Ops:
  12.4 20.1 %collective-permute-done = bf16[512,3,512]{0,2,1:T(8,128)(2,1)} collective-permute-done((bf16[512,3,512]{0,2,1:T(8,128)(2,1)S(1)}, bf16[512,3,512]{0,2,1:T(8,128)(2,1)}, u32[]{:S(2)}, u32[]{:S(2)}) %collective-permute-start) | collective-permute-done | bytes 1572896 | tf_op jit(solution)/shard_map/ppermute | solution.py:16
  33.9 6.6 %all-to-all-start = ((bf16[128,8,512]{0,2,1:T(8,128)(2,1)}), bf16[128,8,512]{0,2,1:T(8,128)(2,1)S(1)}, u32[]{:S(2)}, u32[]{:S(2)}) async-start(bf16[128,8,512]{0,2,1:T(8,128)(2,1)} %bitcast.189), calls=%async_computation | async-start | bytes 2097152 | tf_op jit(solution)/shard_map/all_to_all | solution.py:111
  40.5 12.2 %collective-permute-done.1 = bf16[512,3,512]{0,2,1:T(8,128)(2,1)} collective-permute-done((bf16[512,3,512]{0,2,1:T(8,128)(2,1)}, bf16[512,3,512]{0,2,1:T(8,128)(2,1)}, u32[]{:S(2)}, u32[]{:S(2)}) %collective-permute-start.1) | collective-permute-done | bytes 1572896 | tf_op jit(solution)/shard_map/ppermute | solution.py:16
  52.9 34.9 %all-to-all-done = bf16[128,8,512]{0,2,1:T(8,128)(2,1)S(1)} async-done(((bf16[128,8,512]{0,2,1:T(8,128)(2,1)}), bf16[128,8,512]{0,2,1:T(8,128)(2,1)S(1)}, u32[]{:S(2)}, u32[]{:S(2)}) %all-to-all-start) | async-done | bytes 1048608 | tf_op jit(solution)/shard_map/all_to_all | solution.py:111
  104.1 3.8 constant_dynamic-slice_fusion
  107.9 10.1 %fusion.93 = bf16[1024,1536]{0,1:T(8,128)(2,1)S(1)} fusion(bf16[2048,1536]{0,1:T(8,128)(2,1)} %bitcast.186, bf16[1,1024,2048]{2,1,0:T(8,128)(2,1)} %all-gather.3.cloned.1.call-done), kind=kOutput, calls=%fused_computation.98 | convolution fusion | flops 6444023808 | bytes 13631488 | tf_op jit(solution)/shard_map/dot_general | solution.py:113
  119.7 2.3 copy.63
  124.6 2.3 copy.54
  126.8 2.3 copy.59
  130.2 33.4 %while.38 = (s32[]{:T(128)}, f32[2,256,256]{2,1,0:T(8,128)S(1)}, bf16[8,2,128,256]{3,2,0,1:T(8,128)(2,1)}, bf16[8,2,128,128]{3,2,1,0:T(8,128)(2,1)}, f32[2]{0:T(...) while((s32[]{:T(128)}, f32[2,256,256]{2,1,0:T(8,128)S(1)}, ...), condition=%wide.region_1.2_spmd.clone.clone.clone, body=%wide.region_0.1_spmd.clone.clone.clone.sunk | while | flops 101646848 | bytes 3435178 | solution.py:82
  165.8 52.0 %while.39 = (s32[]{:T(128)}, f32[2,256,256]{2,1,0:T(8,128)S(1)}, bf16[8,2,128,256]{3,2,0,1:T(8,128)(2,1)}, bf16[8,2,128,256]{3,2,0,1:T(8,128)(2,1)}, f32[2]{0:T(...) while((s32[]{:T(128)}, f32[2,256,256]{2,1,0:T(8,128)S(1)}, ...), condition=%wide.region_3.4_spmd.clone.clone.clone, body=%wide.region_2.3_spmd.clone.clone.clone.sunk | while | flops 152306176 | bytes 4880586 | solution.py:83
  169.2 1.8 fusion.138
  175.7 1.8 fusion.138
  182.2 1.8 fusion.138
  188.7 1.8 fusion.138
  195.2 1.8 fusion.138
  201.7 1.8 fusion.138
  208.2 1.8 fusion.138
  214.7 1.8 fusion.138
  222.2 10.5 %fusion.86 = bf16[2048,1536]{0,1:T(8,128)(2,1)} fusion(bf16[1,1024,2048]{2,1,0:T(8,128)(2,1)} %all-gather.3.cloned.1.call-done, bf16[1024,512]{0,1:T(8,128)(2,1)S(1)} %bitcast.200, bf16[1024,512]{0,1:T(8,128)(2,1)S(1)} %bitcast.202, bf16[1024,512]{0,1:T(8,128)(2,1)} %bitcast.204), kind=kOutput, calls=%fused_computation.92 | convolution fusion | flops 6455033856 | bytes 13631488 | tf_op jit(solution)/shard_map/dot_general | solution.py:131
  233.8 11.1 %convolution_convert_fusion.1 = bf16[1024,2048]{1,0:T(8,128)(2,1)} fusion(bf16[2048,1536]{0,1:T(8,128)(2,1)} %bitcast.187, bf16[1024,512]{0,1:T(8,128)(2,1)S(1)} %bitcast.201, bf16[1024,512]{0,1:T(8,128)(2,1)S(1)} %bitcast.203, bf16[1024,512]{0,1:T(8,128)(2,1)S(1)} %bitcast.205), kind=kOutput, calls=%fused_computation.96 | convolution fusion | flops 6453985280 | bytes 13631488 | tf_op jit(solution)/shard_map/dot_general | solution.py:122
  245.0 50.2 %reduce-scatter.5.cloned.1.call-done = bf16[512,1536]{0,1:T(8,128)(2,1)} async-done(((bf16[2048,1536]{0,1:T(8,128)(2,1)}), bf16[512,1536]{0,1:T(8,128)(2,1)}) %reduce-scatter.5.cloned.1.call-update) | async-done | bytes 1572880 | tf_op jit(solution)/shard_map/reduce_scatter | solution.py:130
  295.2 1.8 convert_multiply_fusion
  301.3 86.4 %reduce-scatter.3.cloned.1.call-done = bf16[128,2048]{1,0:T(8,128)(2,1)} async-done(((bf16[1024,2048]{1,0:T(8,128)(2,1)}), bf16[128,2048]{1,0:T(8,128)(2,1)}) %reduce-scatter.3.cloned.1.call-update) | async-done | bytes 524304 | tf_op jit(solution)/shard_map/reduce_scatter | solution.py:121
  (141 shorter events, 110.6 us)
Async XLA Ops:
  7.2 25.4 %copy-start.3 = (bf16[1,128,4096]{2,1,0:T(8,128)(2,1)S(1)}, bf16[1,128,4096]{2,1,0:T(8,128)(2,1)}, u32[]{:S(2)}) copy-start(bf16[1,128,4096]{2,1,0:T(8,128)(2,1)} %param.11) | copy-start | bytes 3145732
  7.2 100.7 %all-gather.3.cloned.1.call-start = ((), (), s32[]{:S(2)}) async-start(), calls=%async_computation.5 | async-start | bytes 4718592 | tf_op jit(solution)/shard_map/all_gather | solution.py:112
  10.4 42.4 %copy-start.5 = (f32[2]{0:T(128)S(1)}, f32[2]{0:T(128)}, u32[]{:S(2)}) copy-start(f32[2]{0:T(128)} %param.15) | copy-start | bytes 28
  11.7 41.1 %copy-start = (bf16[512,512]{0,1:T(8,128)(2,1)}, bf16[512,512]{0,1:T(8,128)(2,1)S(1)}, u32[]{:S(2)}) copy-start(bf16[512,512]{0,1:T(8,128)(2,1)S(1)} %copy.50) | copy-start | bytes 1572868
  11.9 20.7 %collective-permute-start = (bf16[512,3,512]{0,2,1:T(8,128)(2,1)S(1)}, bf16[512,3,512]{0,2,1:T(8,128)(2,1)}, u32[]{:S(2)}, u32[]{:S(2)}) collective-permute-start(bf16[512,3,512]{0,2,1:T(8,128)(2,1)S(1)} %pad_maximum_fusion.1), channel_id=1, source_target_pairs={{0,1},{1,2},{2,3},{3,0},{4,5},{5,6},{6,7},{7,4},{8,9},{9,10},{10,1... | collective-permute-start | bytes 4718600 | tf_op jit(solution)/shard_map/ppermute | solution.py:16
  32.6 20.2 %collective-permute-start.1 = (bf16[512,3,512]{0,2,1:T(8,128)(2,1)}, bf16[512,3,512]{0,2,1:T(8,128)(2,1)}, u32[]{:S(2)}, u32[]{:S(2)}) collective-permute-start(bf16[512,3,512]{0,2,1:T(8,128)(2,1)} %collective-permute-done), channel_id=1, source_target_pairs={{0,1},{1,2},{2,3},{3,0},{4,5},{5,6},{6,7},{7,4},{8,9},{9,10},{10,1... | collective-permute-start | bytes 4718600 | tf_op jit(solution)/shard_map/ppermute | solution.py:16
  33.9 53.9 %all-to-all-start = ((bf16[128,8,512]{0,2,1:T(8,128)(2,1)}), bf16[128,8,512]{0,2,1:T(8,128)(2,1)S(1)}, u32[]{:S(2)}, u32[]{:S(2)}) async-start(bf16[128,8,512]{0,2,1:T(8,128)(2,1)} %bitcast.189), calls=%async_computation | async-start | bytes 2097152 | tf_op jit(solution)/shard_map/all_to_all | solution.py:111
  40.5 254.7 %reduce-scatter.5.cloned.1.call-start = ((), (), s32[]{:S(2)}) async-start(), calls=%async_computation.4 | async-start | bytes 7864320 | tf_op jit(solution)/shard_map/reduce_scatter | solution.py:130
  52.8 40.9 %collective-permute-start.2 = (bf16[512,3,512]{0,2,1:T(8,128)(2,1)}, bf16[512,3,512]{0,2,1:T(8,128)(2,1)}, u32[]{:S(2)}, u32[]{:S(2)}) collective-permute-start(bf16[512,3,512]{0,2,1:T(8,128)(2,1)} %collective-permute-done.1), channel_id=1, source_target_pairs={{0,1},{1,2},{2,3},{3,0},{4,5},{5,6},{6,7},{7,4},{8,9},{9,10},{10,1... | collective-permute-start | bytes 4718600 | tf_op jit(solution)/shard_map/ppermute | solution.py:16
  93.6 5.1 %copy-start.1 = (bf16[512,512]{0,1:T(8,128)(2,1)S(1)}, bf16[512,512]{0,1:T(8,128)(2,1)}, u32[]{:S(2)}) copy-start(bf16[512,512]{0,1:T(8,128)(2,1)} %copy-done) | copy-start | bytes 1572868
  217.7 3.1 copy-start.2
  232.6 1.2 copy-start.4
  232.6 155.1 %reduce-scatter.3.cloned.1.call-start = ((), (), s32[]{:S(2)}) async-start(), calls=%async_computation.3 | async-start | bytes 4718592 | tf_op jit(solution)/shard_map/reduce_scatter | solution.py:121
Sparse Core Ops, SparseCore 0:
  10.1 92.2 all-gather.2
  232.8 62.4 reduce-scatter.4
  299.4 88.2 reduce-scatter.2
